TPU v7x, 32 devices: a whole 2x2x4 slice. The times are simulated.
32 devices in a mesh: grp: 2 (over y), sp: 8 (over z, core), tp: 2 (over x).
Axes of the slice: x: 2, y: 2, z: 4, core: 2. Of those that a mesh axis runs over, the one named last changes fastest.
Arguments:
- resid: bfloat16 [3072, 2048], P(('grp', 'sp', 'tp')), parts along dimension 0, may hold values from -6 to 6
- queries: bfloat16 [3072, 1024], P(('grp', 'sp'), 'tp'), parts along dimension 0, may hold values from -64 to 64
- keys: bfloat16 [3072, 256], P(('grp', 'sp'), 'tp'), parts along dimension 0, may hold values from -64 to 64
- values: bfloat16 [3072, 256], P(('grp', 'sp'), 'tp'), parts along dimension 0, may hold values from -6 to 6
- doc_ids: int32 [3072], P(('grp', 'sp')), parts along dimension 0, may hold values from 0 to 3, never falling along the last dimension, each value on 1 to 768 neighbouring positions
- sink_logits: float32 [16], P('tp'), may hold values from 2 to 6
- out_proj: bfloat16 [1024, 2048], P('tp'), may hold values from -1.5 to 1.5
- norm1_gain: float32 [2048], replicated, may hold values from 0.1 to 1.9
- norm1_bias: float32 [2048], replicated, may hold values from -1.8 to 1.8
- route_ids: int32 [3072, 2], P(('grp', 'sp', 'tp')), parts along dimension 0, may hold values from 0 to 7, all different within a row; in each aligned block of 96 rows (0 to 95, 96 to 191, ...) at most 30 rows name the same one
- route_weights: float32 [3072, 2], P(('grp', 'sp', 'tp')), parts along dimension 0, may hold values from 0.25 to 1
- expert_gate: bfloat16 [8, 2048, 3072], P('sp', None, 'tp'), may hold values from -0.125 to 0.125
- expert_up: bfloat16 [8, 2048, 3072], P('sp', None, 'tp'), may hold values from -0.125 to 0.125
- expert_down: bfloat16 [8, 3072, 2048], P('sp', 'tp'), may hold values from -0.109375 to 0.109375
- norm2_gain: float32 [2048], replicated, may hold values from 0.1 to 1.9
- norm2_bias: float32 [2048], replicated, may hold values from -1.8 to 1.8
Outputs:
- mixed: bfloat16 [3072, 2048], P(('grp', 'sp', 'tp')), parts along dimension 0
There are 2 independent parts, one for each index of `grp`. A program takes and returns all parts, laid end to end along the dimension named above; an argument that names none is the same for every part. Nothing has to cross between parts.
Inputs may be any that keep to these rules, and one draw needn't show every extreme that they name: `route_ids`: among the rows of one device (aligned blocks of 96 tokens) no expert is named more than 30 times, a bound that some block reaches; a token's 2 experts differ.
All inputs are finite; a program needn't handle non-finite values.
Results may differ from a plain program's by a relative error of at most 0.012.
Values may be sent and summed in bfloat16 or wider, within the bound.
A program may use at most 64 MiB of HBM per device.

v0:
```python
import jax
import jax.numpy as jnp
from jax import lax
from jax.sharding import PartitionSpec as P

HEAD_DIM = 64
WINDOW = 128


norm_epsilon = 1e-05
residual_scale = 1.4142135623730951
masked_score = -1e30


def with_halo(cells, sides, width):
    for axis, dim in sides:
        count = lax.axis_size(axis)
        ends = count - 1
        head = lax.slice_in_dim(cells, 0, width, axis=dim)
        tail = lax.slice_in_dim(cells, cells.shape[dim] - width, cells.shape[dim], axis=dim)
        cells = jnp.concatenate(
            [
                lax.ppermute(tail, axis, [(i, (i + 1) % count) for i in range(ends)]),
                cells,
                lax.ppermute(head, axis, [((i + 1) % count, i) for i in range(ends)]),
            ],
            axis=dim,
        )
    return cells


def layer_norm(values, gain_vec, bias_vec):
    mean_val = jnp.mean(values, -1, keepdims=True)
    centred = values - mean_val
    variance = jnp.mean(centred * centred, -1, keepdims=True)
    return centred * lax.rsqrt(variance + norm_epsilon) * gain_vec + bias_vec


def per_device(
    resid,
    queries,
    keys,
    values,
    doc_ids,
    sink_logits,
    out_proj,
    norm1_gain,
    norm1_bias,
    route_ids,
    route_weights,
    expert_gate,
    expert_up,
    expert_down,
    norm2_gain,
    norm2_bias,
):
    tok_dev = queries.shape[0]
    local_kv = keys.shape[1] // HEAD_DIM
    local_heads = queries.shape[1] // HEAD_DIM
    groups = local_heads // local_kv
    reach = tok_dev + 2 * WINDOW
    padded_keys, padded_values, padded_docs = (
        with_halo(keys, (("sp", 0),), WINDOW),
        with_halo(values, (("sp", 0),), WINDOW),
        with_halo(doc_ids, (("sp", 0),), WINDOW),
    )
    offset = lax.axis_index("sp") * tok_dev
    seq_total = lax.axis_size("sp") * tok_dev
    query_pos = offset + jnp.arange(tok_dev, dtype=jnp.int32)
    key_pos = offset - WINDOW + jnp.arange(reach, dtype=jnp.int32)
    allowed = (key_pos[None, :] >= 0) & (key_pos[None, :] < seq_total)
    allowed = allowed & (jnp.abs(query_pos[:, None] - key_pos[None, :]) <= WINDOW)
    allowed = allowed & (doc_ids[:, None] == padded_docs[None, :])
    query_heads = queries.reshape(tok_dev, local_kv, groups, HEAD_DIM)
    key_heads = padded_keys.reshape(reach, local_kv, HEAD_DIM)
    value_heads = padded_values.reshape(reach, local_kv, HEAD_DIM)
    sink_local = sink_logits.reshape(local_kv, groups, 1, 1)
    scores = jnp.einsum(
        "qkgd,jkd->kgqj", query_heads, key_heads, preferred_element_type=jnp.float32
    )
    scores = jnp.where(allowed, scores * HEAD_DIM ** (-0.5), masked_score)
    top_score = jnp.maximum(jnp.max(scores, -1, keepdims=True), sink_local)
    raised = jnp.where(allowed, jnp.exp(scores - top_score), 0.0)
    denominator = jnp.exp(sink_local - top_score) + jnp.sum(raised, -1, keepdims=True)
    weights = (raised / denominator).astype(jnp.bfloat16)
    attended = jnp.einsum(
        "kgqj,jkd->qkgd", weights, value_heads, preferred_element_type=jnp.float32
    )
    attended = attended.astype(jnp.bfloat16).reshape(tok_dev, local_heads * HEAD_DIM)
    tp_size = lax.axis_size("tp")
    tok_sub = resid.shape[0]
    row_block = attended
    projected = lax.psum_scatter(
        jnp.dot(row_block, out_proj, preferred_element_type=jnp.float32).astype(jnp.bfloat16),
        "tp",
        scatter_dimension=0,
        tiled=True,
    )
    pre_norm = residual_scale * resid.astype(jnp.float32) + projected.astype(jnp.float32)
    normed = layer_norm(pre_norm, norm1_gain, norm1_bias).astype(jnp.bfloat16)
    experts = lax.axis_size("sp")
    capacity = 5 * tok_sub // (2 * experts)
    width = normed.shape[1]
    flat_ids = route_ids.reshape(-1)
    one_hot = (flat_ids[:, None] == jnp.arange(experts, dtype=jnp.int32)[None, :]).astype(jnp.int32)
    ranks = jnp.cumsum(one_hot, axis=0) - 1
    slot_rank = jnp.sum(ranks * one_hot, axis=1)
    slots = flat_ids * capacity + slot_rank
    assignment = slots[None, :] == jnp.arange(experts * capacity, dtype=jnp.int32)[:, None]
    assignment = assignment.reshape(experts * capacity, tok_sub, -1).any(-1).astype(jnp.bfloat16)
    dispatch = jnp.dot(assignment, normed, preferred_element_type=jnp.float32).astype(jnp.bfloat16)
    dispatch = dispatch.reshape(experts, capacity, width)
    copies = jnp.broadcast_to(dispatch[:, None], (experts, tp_size, capacity, width))
    copies = copies.reshape(experts * tp_size, capacity, width)
    arrived = lax.all_to_all(copies, ("sp", "tp"), split_axis=0, concat_axis=0, tiled=True)
    arrived = arrived.reshape(experts, tp_size, capacity, width).transpose(1, 0, 2, 3)
    flat_rows = arrived.reshape(-1, width)
    gate_weight = expert_gate[0]
    up_weight = expert_up[0]
    down_weight = expert_down[0]
    row_block = flat_rows
    gate_act = jnp.dot(row_block, gate_weight, preferred_element_type=jnp.float32)
    up_act = jnp.dot(row_block, up_weight, preferred_element_type=jnp.float32)
    hidden = (jax.nn.silu(gate_act) * up_act).astype(jnp.bfloat16)
    expert_out = lax.psum_scatter(
        jnp.dot(hidden, down_weight, preferred_element_type=jnp.float32).astype(jnp.bfloat16),
        "tp",
        scatter_dimension=0,
        tiled=True,
    )
    returned = lax.all_to_all(
        expert_out.reshape(experts, capacity, width), "sp", split_axis=0, concat_axis=0, tiled=True
    )
    gathered = jnp.take(returned.reshape(experts * capacity, width), slots, axis=0)
    gathered = gathered.reshape(tok_sub, -1, width).astype(jnp.float32)
    moe_sum = jnp.sum(route_weights[:, :, None] * gathered, axis=1)
    pre_final = residual_scale * normed.astype(jnp.float32) + moe_sum
    return layer_norm(pre_final, norm2_gain, norm2_bias).astype(jnp.bfloat16)


def solution(mesh):
    return jax.shard_map(
        per_device,
        mesh=mesh,
        in_specs=(
            P(("grp", "sp", "tp"), None),
            P(("grp", "sp"), "tp"),
            P(("grp", "sp"), "tp"),
            P(("grp", "sp"), "tp"),
            P(("grp", "sp")),
            P("tp"),
            P("tp", None),
            P(),
            P(),
            P(("grp", "sp", "tp"), None),
            P(("grp", "sp", "tp"), None),
            P("sp", None, "tp"),
            P("sp", None, "tp"),
            P("sp", "tp", None),
            P(),
            P(),
        ),
        out_specs=P(("grp", "sp", "tp"), None),
        check_vma=False,
    )
```

profile of v0, /device:TPU:0, one launch (start us, length us, event | category | flops | bytes accessed | tf_op | source)
XLA Modules:
  0.0 229.1 jit_solution(7260586472731464765)
XLA Ops:
  6.5 0.9 fusion.36
  7.5 2.4 %collective-permute-start.2 = (s32[128]{0:T(128)S(1)}, s32[128]{0:T(128)S(1)}, u32[]{:S(2)}, u32[]{:S(2)}) collective-permute-start(s32[128]{0:T(128)S(1)} %get-tuple-element.11), channel_id=1, source_target_pairs={{0,2},{2,4},{4,6},{6,8},{8,10},{10,12},{12,14},{1,3},{3,5},{5,7},{... | collective-permute-start | bytes 1544 | tf_op jit(solution)/shard_map/ppermute | solution.py:23
  9.8 1.3 collective-permute-start.3
  11.1 0.8 fusion.34
  12.0 5.2 %collective-permute-start.4 = (bf16[128,128]{1,0:T(8,128)(2,1)S(1)}, bf16[128,128]{1,0:T(8,128)(2,1)S(1)}, u32[]{:S(2)}, u32[]{:S(2)}) collective-permute-start(bf16[128,128]{1,0:T(8,128)(2,1)S(1)} %get-tuple-element.7), channel_id=1, source_target_pairs={{0,2},{2,4},{4,6},{6,8},{8,10},{10,12},{12,14},{1,3},{3,5},{5,7},{... | collective-permute-start | bytes 98312 | tf_op jit(solution)/shard_map/ppermute | solution.py:23
  17.2 1.3 collective-permute-start.5
  18.5 0.8 fusion.35
  19.3 4.3 %collective-permute-start = (bf16[128,128]{1,0:T(8,128)(2,1)S(1)}, bf16[128,128]{1,0:T(8,128)(2,1)S(1)}, u32[]{:S(2)}, u32[]{:S(2)}) collective-permute-start(bf16[128,128]{1,0:T(8,128)(2,1)S(1)} %get-tuple-element.9), channel_id=1, source_target_pairs={{0,2},{2,4},{4,6},{6,8},{8,10},{10,12},{12,14},{1,3},{3,5},{5,7},{... | collective-permute-start | bytes 98312 | tf_op jit(solution)/shard_map/ppermute | solution.py:23
  23.7 1.1 copy.56
  24.7 0.7 max.18
  25.5 1.3 collective-permute-start.1
  26.8 0.8 pad_add_fusion
  27.5 0.9 fusion.23
  28.4 0.8 pad_maximum_fusion.1
  29.3 0.1 copy.55
  29.4 0.9 fusion.15
  30.3 0.1 broadcast_maximum_fusion
  30.3 1.6 copy-done.1
  31.9 1.1 fusion.16
  33.0 0.1 exponential_add_fusion
  33.2 0.1 copy.54
  33.3 3.0 %fusion.18 = bf16[2,64,4,192]{3,1,2,0:T(8,128)(2,1)S(1)} fusion(bf16[448,2,64,1]{0,2,3,1:T(8,128)(2,1)S(1)} %bitcast.72, f32[2,448,192,4]{1,2,3,0:T(8,128)} %copy-done.1, f32[2,4,192]{2,1,0:T(4,128)S(1)} %exponential_add_fusion, f32[2,4,192]{2,1,0:T(4,128)S(1)} %broadcast_maximum_fusion, pred[192,448]{1,0:T(8,128)(4,1)S(1)} %fusion.23), kind=kOutput, calls=%fused_computation.21 | convolution fusion | flops 92307456 | bytes 3162112 | tf_op jit(solution)/shard_map/kgqj,jkd->qkgd/dot_general | solution.py:86
  36.3 0.0 copy-start.2
  36.3 0.0 copy-start.5
  36.4 1.5 convolution_convert_fusion.1
  37.9 0.0 reduce-scatter.3.cloned.1.call-update
  37.9 0.0 reduce-scatter.5.cloned.1.call-start
  38.0 0.1 copy.58
  38.1 0.1 reshape.171
  38.2 0.6 reduce-window.6
  38.8 0.2 slice_reduce_fusion
  39.1 0.1 add_bitcast_fusion
  39.2 0.1 reduce_sum.71
  39.3 0.1 copy.59
  39.4 0.1 fusion.25
  39.5 19.7 %reduce-scatter.3.cloned.1.call-done = bf16[96,2048]{1,0:T(8,128)(2,1)} async-done(((bf16[192,2048]{1,0:T(8,128)(2,1)}), bf16[96,2048]{1,0:T(8,128)(2,1)}) %reduce-scatter.3.cloned.1.call-update) | async-done | bytes 393232 | tf_op jit(solution)/shard_map/reduce_scatter | solution.py:93
  59.2 1.2 fusion.21
  60.5 1.3 multiply_reduce_fusion.2
  61.8 1.2 add_convert_fusion.1
  63.0 1.4 convolution_convert_fusion
  64.4 1.5 broadcast_in_dim.30
  65.9 0.2 broadcast_in_dim.31
  66.2 52.8 %all_to_all.10 = bf16[16,30,2048]{2,1,0:T(8,128)(2,1)S(1)} all-to-all(bf16[16,30,2048]{2,1,0:T(8,128)(2,1)S(1)} %bitcast.66), channel_id=1, replica_groups=mesh['grp'=2,'sp'=8,'tp'=2] {'sp','tp'}, dimensions={0} | all-to-all | bytes 3932160 | tf_op jit(solution)/shard_map/all_to_all | solution.py:115
  119.0 2.0 copy.68
  121.0 2.4 %copy.62 = bf16[2,8,30,2048]{3,2,1,0:T(8,128)(2,1)} copy(bf16[2,8,30,2048]{3,0,1,2:T(2,128)(2,1)S(1)} %bitcast.68) | data formatting | bytes 3932160 | tf_op jit(solution)/shard_map/transpose | solution.py:116
  123.4 2.8 %reshape.176 = bf16[480,2048]{1,0:T(8,128)(2,1)} reshape(bf16[2,8,30,2048]{3,2,1,0:T(8,128)(2,1)} %copy.62) | data formatting | bytes 3932160 | tf_op jit(solution)/shard_map/reshape | solution.py:117
  126.2 8.2 %fusion.4 = f32[480,1536]{1,0:T(8,128)} fusion(bf16[480,2048]{1,0:T(8,128)(2,1)} %reshape.176, bf16[1,2048,1536]{2,1,0:T(8,128)(2,1)} %param.27), kind=kOutput, calls=%fused_computation.5 | convolution fusion | flops 3019898880 | bytes 11206656 | tf_op jit(solution)/shard_map/dot_general | solution.py:122
  134.4 13.7 %fusion.12 = bf16[480,2048]{1,0:T(8,128)(2,1)} fusion(bf16[1,1536,2048]{2,1,0:T(8,128)(2,1)} %param.29, bf16[480,2048]{1,0:T(8,128)(2,1)} %reshape.176, bf16[1,2048,1536]{2,1,0:T(8,128)(2,1)} %param.28, f32[480,1536]{1,0:T(8,128)} %fusion.4), kind=kOutput, calls=%fused_computation.12 | convolution fusion | flops 6045204480 | bytes 19464192 | tf_op jit(solution)/shard_map/dot_general | solution.py:126
  148.1 0.0 reduce-scatter.5.cloned.1.call-update
  148.1 29.9 %reduce-scatter.5.cloned.1.call-done = bf16[240,2048]{1,0:T(8,128)(2,1)} async-done(((bf16[480,2048]{1,0:T(8,128)(2,1)}), bf16[240,2048]{1,0:T(8,128)(2,1)}) %reduce-scatter.5.cloned.1.call-update) | async-done | bytes 983056 | tf_op jit(solution)/shard_map/reduce_scatter | solution.py:125
  178.0 2.5 %reshape.177 = bf16[8,30,2048]{2,1,0:T(8,128)(2,1)} reshape(bf16[240,2048]{1,0:T(8,128)(2,1)} %reduce-scatter.5.cloned.1.call-done) | data formatting | bytes 1966080 | tf_op jit(solution)/shard_map/reshape | solution.py:132
  180.5 4.6 %all-to-all-start.1 = ((bf16[8,30,2048]{2,1,0:T(8,128)(2,1)}), bf16[8,30,2048]{2,1,0:T(8,128)(2,1)}, u32[]{:S(2)}, u32[]{:S(2)}) async-start(bf16[8,30,2048]{2,1,0:T(8,128)(2,1)} %reshape.177), calls=%async_computation.3 | async-start | bytes 2097152 | tf_op jit(solution)/shard_map/all_to_all | solution.py:131
  185.1 0.1 copy.63
  185.2 0.1 mul.114
  185.4 0.1 copy.60
  185.5 0.1 copy.57
  185.6 26.2 %all-to-all-done.1 = bf16[8,30,2048]{2,1,0:T(8,128)(2,1)} async-done(((bf16[8,30,2048]{2,1,0:T(8,128)(2,1)}), bf16[8,30,2048]{2,1,0:T(8,128)(2,1)}, u32[]{:S(2)}, u32[]{:S(2)}) %all-to-all-start.1) | async-done | bytes 983072 | tf_op jit(solution)/shard_map/all_to_all | solution.py:131
  211.8 1.5 reshape.178
  213.3 2.0 gather_fusion
  215.3 2.2 gather.7
  217.5 3.3 %multiply_reduce_fusion = f32[96,2048]{1,0:T(8,128)S(1)} fusion(bf16[96,2,2048]{2,1,0:T(2,128)(2,1)S(1)} %gather.7, pred[96,2]{1,0:T(8,128)(4,1)S(1)} %copy.60, f32[96,2]{1,0:T(8,128)S(1)} %copy.57), kind=kLoop, calls=%fused_computation.18 | loop fusion | flops 1376256 | bytes 1573824 | tf_op jit(solution)/shard_map/reduce_sum | solution.py:136
  220.8 0.2 fusion.24
  221.0 0.3 multiply_reduce_fusion.1
  221.3 1.0 add_convert_fusion
  (41 shorter events, 0.2 us)
Async XLA Ops:
  6.5 29.8 %copy-start = (bf16[512,2048]{1,0:T(8,128)(2,1)S(1)}, bf16[512,2048]{1,0:T(8,128)(2,1)}, u32[]{:S(2)}) copy-start(bf16[512,2048]{1,0:T(8,128)(2,1)} %param.22) | copy-start | bytes 6291460
  6.5 52.7 %reduce-scatter.3.cloned.1.call-start = ((), (), s32[]{:S(2)}) async-start(), calls=%async_computation.4 | async-start | bytes 1179648 | tf_op jit(solution)/shard_map/reduce_scatter | solution.py:93
  7.5 18.0 %collective-permute-start.2 = (s32[128]{0:T(128)S(1)}, s32[128]{0:T(128)S(1)}, u32[]{:S(2)}, u32[]{:S(2)}) collective-permute-start(s32[128]{0:T(128)S(1)} %get-tuple-element.11), channel_id=1, source_target_pairs={{0,2},{2,4},{4,6},{6,8},{8,10},{10,12},{12,14},{1,3},{3,5},{5,7},{... | collective-permute-start | bytes 1544 | tf_op jit(solution)/shard_map/ppermute | solution.py:23
  9.8 16.9 %collective-permute-start.3 = (s32[128]{0:T(128)S(1)}, s32[128]{0:T(128)S(1)}, u32[]{:S(2)}, u32[]{:S(2)}) collective-permute-start(s32[128]{0:T(128)S(1)} %get-tuple-element.12), channel_id=1, source_target_pairs={{2,0},{4,2},{6,4},{8,6},{10,8},{12,10},{14,12},{3,1},{5,3},{7,5},{... | collective-permute-start | bytes 1544 | tf_op jit(solution)/shard_map/ppermute | solution.py:25
  12.0 16.4 %collective-permute-start.4 = (bf16[128,128]{1,0:T(8,128)(2,1)S(1)}, bf16[128,128]{1,0:T(8,128)(2,1)S(1)}, u32[]{:S(2)}, u32[]{:S(2)}) collective-permute-start(bf16[128,128]{1,0:T(8,128)(2,1)S(1)} %get-tuple-element.7), channel_id=1, source_target_pairs={{0,2},{2,4},{4,6},{6,8},{8,10},{10,12},{12,14},{1,3},{3,5},{5,7},{... | collective-permute-start | bytes 98312 | tf_op jit(solution)/shard_map/ppermute | solution.py:23
  17.2 11.2 %collective-permute-start.5 = (bf16[128,128]{1,0:T(8,128)(2,1)S(1)}, bf16[128,128]{1,0:T(8,128)(2,1)S(1)}, u32[]{:S(2)}, u32[]{:S(2)}) collective-permute-start(bf16[128,128]{1,0:T(8,128)(2,1)S(1)} %get-tuple-element.8), channel_id=1, source_target_pairs={{2,0},{4,2},{6,4},{8,6},{10,8},{12,10},{14,12},{3,1},{5,3},{7,5},{... | collective-permute-start | bytes 98312 | tf_op jit(solution)/shard_map/ppermute | solution.py:25
  19.3 13.8 %collective-permute-start = (bf16[128,128]{1,0:T(8,128)(2,1)S(1)}, bf16[128,128]{1,0:T(8,128)(2,1)S(1)}, u32[]{:S(2)}, u32[]{:S(2)}) collective-permute-start(bf16[128,128]{1,0:T(8,128)(2,1)S(1)} %get-tuple-element.9), channel_id=1, source_target_pairs={{0,2},{2,4},{4,6},{6,8},{8,10},{10,12},{12,14},{1,3},{3,5},{5,7},{... | collective-permute-start | bytes 98312 | tf_op jit(solution)/shard_map/ppermute | solution.py:23
  25.5 7.7 %collective-permute-start.1 = (bf16[128,128]{1,0:T(8,128)(2,1)S(1)}, bf16[128,128]{1,0:T(8,128)(2,1)S(1)}, u32[]{:S(2)}, u32[]{:S(2)}) collective-permute-start(bf16[128,128]{1,0:T(8,128)(2,1)S(1)} %get-tuple-element.10), channel_id=1, source_target_pairs={{2,0},{4,2},{6,4},{8,6},{10,8},{12,10},{14,12},{3,1},{5,3},{7,5},{... | collective-permute-start | bytes 98312 | tf_op jit(solution)/shard_map/ppermute | solution.py:25
  29.4 3.8 %copy-start.3 = (bf16[192,128]{1,0:T(8,128)(2,1)S(1)}, bf16[192,128]{1,0:T(8,128)(2,1)}, u32[]{:S(2)}) copy-start(bf16[192,128]{1,0:T(8,128)(2,1)} %param.19) | copy-start | bytes 147460
  30.3 1.7 copy-start.1
  36.3 1.6 copy-start.4
  36.3 22.9 %copy-start.2 = (bf16[96,2048]{1,0:T(8,128)(2,1)S(1)}, bf16[96,2048]{1,0:T(8,128)(2,1)}, u32[]{:S(2)}) copy-start(bf16[96,2048]{1,0:T(8,128)(2,1)} %param.16) | copy-start | bytes 1179652
  36.3 25.4 %copy-start.5 = (f32[2048]{0:T(1024)S(1)}, f32[2048]{0:T(1024)}, u32[]{:S(2)}) copy-start(f32[2048]{0:T(1024)} %param.24) | copy-start | bytes 24580
  36.4 25.4 %copy-start.6 = (f32[2048]{0:T(1024)S(1)}, f32[2048]{0:T(1024)}, u32[]{:S(2)}) copy-start(f32[2048]{0:T(1024)} %param.23) | copy-start | bytes 24580
  37.9 140.1 %reduce-scatter.5.cloned.1.call-start = ((), (), s32[]{:S(2)}) async-start(), calls=%async_computation.5 | async-start | bytes 2949120 | tf_op jit(solution)/shard_map/reduce_scatter | solution.py:125
  148.1 37.4 %copy-start.9 = (f32[96,2]{0,1:T(2,128)S(1)}, f32[96,2]{0,1:T(2,128)}, u32[]{:S(2)}) copy-start(f32[96,2]{0,1:T(2,128)} %param.26) | copy-start | bytes 2308
  180.5 31.3 %all-to-all-start.1 = ((bf16[8,30,2048]{2,1,0:T(8,128)(2,1)}), bf16[8,30,2048]{2,1,0:T(8,128)(2,1)}, u32[]{:S(2)}, u32[]{:S(2)}) async-start(bf16[8,30,2048]{2,1,0:T(8,128)(2,1)} %reshape.177), calls=%async_computation.3 | async-start | bytes 2097152 | tf_op jit(solution)/shard_map/all_to_all | solution.py:131
  215.3 6.0 %copy-start.7 = (f32[2048]{0:T(1024)S(1)}, f32[2048]{0:T(1024)}, u32[]{:S(2)}) copy-start(f32[2048]{0:T(1024)} %param.31) | copy-start | bytes 24580
  215.3 6.0 %copy-start.8 = (f32[2048]{0:T(1024)S(1)}, f32[2048]{0:T(1024)}, u32[]{:S(2)}) copy-start(f32[2048]{0:T(1024)} %param.30) | copy-start | bytes 24580
Sparse Core Ops, SparseCore 0:
  38.0 21.1 reduce-scatter.2
  148.2 29.7 reduce-scatter.4
where the time goes:
time: 230 us; the launch traced here: 229 us
  waiting for transfers between devices  75.9 us (33%)
  blocking collectives  52.8 us (23%)
  matrix products  28.7 us (12%)
  local copies, waits for them, and re-layouts  24.5 us (11%)
  starting transfers between devices  20.4 us (9%)
  between operations  13.8 us (6%)
  other arithmetic  13.1 us (6%)
    all_to_all x1, blocking collectives, per_device(): lax.all_to_all(copies, ('sp', 'tp'), split_axis=0, concat_axis=0, tiled=T...  52.8 us
    reduce_scatter x1, waiting for transfers between devices, per_device(): lax.psum_scatter(jnp.dot(hidden, down_weight, preferred_element_type=jnp....  29.9 us
    all_to_all x1, waiting for transfers between devices, per_device(): lax.all_to_all(expert_out.reshape(experts, capacity, width), 'sp', split_...  26.2 us
    reduce_scatter x1, waiting for transfers between devices, per_device(): lax.psum_scatter(jnp.dot(row_block, out_proj, preferred_element_type=jnp....  19.7 us
    dot_general x1, matrix products, per_device(): jnp.dot(hidden, down_weight, preferred_element_type=jnp.float32)  13.7 us
    ppermute x3, starting transfers between devices, with_halo(): lax.ppermute(tail, axis, [(i, (i + 1) % count) for i in range(ends)])  11.8 us
    dot_general x1, matrix products, per_device(): jnp.dot(row_block, gate_weight, preferred_element_type=jnp.float32)  8.19 us
    all_to_all x1, starting transfers between devices, per_device(): lax.all_to_all(expert_out.reshape(experts, capacity, width), 'sp', split_...  4.62 us
  transfers between devices with their start and end apart: 9, of which 3 were waited for; matrix products, arithmetic and copies ran while one was open for 4% of the time, Pallas kernels for 0%

commit v1 on v0

--- a/solution.py
+++ b/solution.py
@@ -1,10 +1,15 @@
+import functools
+
 import jax
 import jax.numpy as jnp
 from jax import lax
+from jax.experimental import pallas as pl
+from jax.experimental.pallas import tpu as pltpu
 from jax.sharding import PartitionSpec as P
 
 HEAD_DIM = 64
 WINDOW = 128
+MESH = pl.DeviceIdType.MESH
 
 
 norm_epsilon = 1e-05
@@ -34,6 +39,287 @@
     centred = values - mean_val
     variance = jnp.mean(centred * centred, -1, keepdims=True)
     return centred * lax.rsqrt(variance + norm_epsilon) * gain_vec + bias_vec
+
+
+def step_partner(step, sp_pos, count, back):
+    chip, core = sp_pos // 2, sp_pos % 2
+    half = count // 4
+    side, place = chip // half, chip % half
+    pair, flip = step // 2, step % 2
+    if pair == 0:
+        turn, cross = 0, False
+    elif pair <= half:
+        turn, cross = pair - 1, True
+    else:
+        turn, cross = pair - half, False
+    target_side = 1 - side if cross else side
+    move = half - turn if back else turn
+    target = target_side * half + (place + move) % half
+    return target * 2 + (core + flip) % 2
+
+
+def moe_kernel(
+    experts,
+    tps,
+    chunk,
+    normed_ref,
+    ids_ref,
+    rw_ref,
+    gain_ref,
+    bias_ref,
+    gate_hbm,
+    up_hbm,
+    down_hbm,
+    out_ref,
+    outgoing,
+    rows,
+    gate_w,
+    up_w,
+    down_w,
+    hidden,
+    part,
+    peer,
+    summed,
+    returned,
+    w_sem,
+    disp_send,
+    disp_recv,
+    fwd_send,
+    fwd_recv,
+    part_send,
+    part_recv,
+    ret_send,
+    ret_recv,
+):
+    me, t = lax.axis_index("sp"), lax.axis_index("tp")
+    _, capacity, width = outgoing.shape
+    toks = normed_ref.shape[0]
+    weight_copies = [
+        pltpu.make_async_copy(gate_hbm.at[0], gate_w, w_sem.at[0]),
+        pltpu.make_async_copy(up_hbm.at[0], up_w, w_sem.at[1]),
+        pltpu.make_async_copy(down_hbm.at[0], down_w, w_sem.at[2]),
+    ]
+    for copy in weight_copies:
+        copy.start()
+
+    barrier = pltpu.get_barrier_semaphore()
+    for d in range(1, experts):
+        pl.semaphore_signal(
+            barrier, inc=1, device_id={"sp": (me + d) % experts}, device_id_type=MESH
+        )
+    for d in range(1, tps):
+        pl.semaphore_signal(barrier, inc=1, device_id={"tp": (t + d) % tps}, device_id_type=MESH)
+
+    lanes = experts * capacity
+    ids = ids_ref[...]
+    wide = max(experts, 128)
+    expert_iota = lax.broadcasted_iota(jnp.int32, (toks, wide), 1)
+    lower = (
+        lax.broadcasted_iota(jnp.int32, (toks, toks), 0)
+        > lax.broadcasted_iota(jnp.int32, (toks, toks), 1)
+    ).astype(jnp.float32).astype(jnp.bfloat16)
+    before = jnp.zeros((1, wide), jnp.float32)
+    slot_iota = lax.broadcasted_iota(jnp.int32, (toks, lanes), 1)
+    assign = jnp.zeros((toks, lanes), jnp.float32)
+    combine = jnp.zeros((toks, lanes), jnp.float32)
+    for k in range(ids.shape[1]):
+        own = ids[:, k : k + 1]
+        hot = (own == expert_iota).astype(jnp.float32)
+        rank = before + jnp.dot(lower, hot.astype(jnp.bfloat16), preferred_element_type=jnp.float32)
+        rank = jnp.sum(rank * hot, axis=1, keepdims=True).astype(jnp.int32)
+        before = before + jnp.sum(hot, axis=0, keepdims=True)
+        match = (own * capacity + rank == slot_iota).astype(jnp.float32)
+        assign = assign + match
+        combine = combine + match * rw_ref[:, k : k + 1]
+    spread = lax.dot_general(
+        assign.astype(jnp.bfloat16),
+        normed_ref[...],
+        (((0,), (0,)), ((), ())),
+        preferred_element_type=jnp.float32,
+    )
+    outgoing[...] = spread.astype(jnp.bfloat16).reshape(experts, capacity, width)
+    rows[0, t] = outgoing[me]
+
+    pl.semaphore_wait(barrier, experts - 1 + tps - 1)
+
+    def dispatch(step):
+        dst = step_partner(step, me, experts, False)
+        return pltpu.make_async_remote_copy(
+            src_ref=outgoing.at[dst],
+            dst_ref=rows.at[step, t],
+            send_sem=disp_send.at[step],
+            recv_sem=disp_recv.at[step],
+            device_id={"sp": dst},
+            device_id_type=MESH,
+        )
+
+    def forward(step, d):
+        dst = (t + d) % tps
+        return pltpu.make_async_remote_copy(
+            src_ref=rows.at[step, t],
+            dst_ref=rows.at[step, t],
+            send_sem=fwd_send.at[step, d],
+            recv_sem=fwd_recv.at[step, d],
+            device_id={"tp": dst},
+            device_id_type=MESH,
+        )
+
+    def share(step, d):
+        dst = (t + d) % tps
+        return pltpu.make_async_remote_copy(
+            src_ref=part.at[step, dst],
+            dst_ref=peer.at[step, d],
+            send_sem=part_send.at[step, d],
+            recv_sem=part_recv.at[step, d],
+            device_id={"tp": dst},
+            device_id_type=MESH,
+        )
+
+    def give_back(step):
+        dst = step_partner(step, me, experts, True)
+        return pltpu.make_async_remote_copy(
+            src_ref=summed.at[step],
+            dst_ref=returned.at[me],
+            send_sem=ret_send.at[step],
+            recv_sem=ret_recv.at[step],
+            device_id={"sp": dst},
+            device_id_type=MESH,
+        )
+
+    for step in range(1, experts):
+        dispatch(step).start()
+
+    def send_on(step):
+        if step > 0:
+            dispatch(step).wait_recv()
+        for d in range(1, tps):
+            forward(step, d).start()
+
+    def finish(step):
+        total = part[step, t].astype(jnp.float32)
+        for d in range(1, tps):
+            share(step, d).wait_recv()
+            total = total + peer[step, d].astype(jnp.float32)
+        if step == 0:
+            returned[me] = total.astype(jnp.bfloat16)
+        else:
+            summed[step] = total.astype(jnp.bfloat16)
+            give_back(step).start()
+
+    tile = 256
+    hidden_width = gate_w.shape[1]
+    m = chunk * tps * capacity
+    chunks = experts // chunk
+
+    for c in range(chunks):
+        k0, k1 = c * chunk, (c + 1) * chunk
+        for step in range(k0, k1):
+            send_on(step)
+        for step in range(k0, k1):
+            for d in range(1, tps):
+                forward(step, d).wait_recv()
+        if c == 0:
+            weight_copies[0].wait()
+            weight_copies[1].wait()
+
+        def up_tile(i, carry):
+            cols = pl.ds(pl.multiple_of(i * tile, tile), tile)
+            block = rows[k0:k1].reshape(m, width)
+            gate = jnp.dot(block, gate_w[:, cols], preferred_element_type=jnp.float32)
+            up = jnp.dot(block, up_w[:, cols], preferred_element_type=jnp.float32)
+            hidden[:, cols] = (gate / (1.0 + jnp.exp(-gate)) * up).astype(jnp.bfloat16)
+            return carry
+
+        lax.fori_loop(0, hidden_width // tile, up_tile, 0)
+        if c == 0:
+            weight_copies[2].wait()
+
+        def down_tile(i, carry):
+            cols = pl.ds(pl.multiple_of(i * tile, tile), tile)
+            result = jnp.dot(hidden[...], down_w[:, cols], preferred_element_type=jnp.float32)
+            part[k0:k1, :, :, cols] = result.astype(jnp.bfloat16).reshape(
+                chunk, tps, capacity, tile
+            )
+            return carry
+
+        lax.fori_loop(0, width // tile, down_tile, 0)
+        for step in range(k0, k1):
+            for d in range(1, tps):
+                share(step, d).start()
+        if c > 0:
+            for step in range(k0 - chunk, k0):
+                finish(step)
+    for step in range(experts - chunk, experts):
+        finish(step)
+    for step in range(1, experts):
+        src = step_partner(step, me, experts, False)
+        pltpu.make_async_remote_copy(
+            src_ref=summed.at[step],
+            dst_ref=returned.at[src],
+            send_sem=ret_send.at[step],
+            recv_sem=ret_recv.at[step],
+            device_id={"sp": src},
+            device_id_type=MESH,
+        ).wait_recv()
+
+    back = returned[...].reshape(lanes, width)
+    high = combine.astype(jnp.bfloat16)
+    low = (combine - high.astype(jnp.float32)).astype(jnp.bfloat16)
+    moe_sum = jnp.dot(high, back, preferred_element_type=jnp.float32)
+    moe_sum = moe_sum + jnp.dot(low, back, preferred_element_type=jnp.float32)
+    pre_final = residual_scale * normed_ref[...].astype(jnp.float32) + moe_sum
+    out_ref[...] = layer_norm(pre_final, gain_ref[...], bias_ref[...]).astype(jnp.bfloat16)
+
+    for step in range(experts):
+        if step > 0:
+            dispatch(step).wait_send()
+            give_back(step).wait_send()
+        for d in range(1, tps):
+            forward(step, d).wait_send()
+            share(step, d).wait_send()
+
+
+def run_moe(normed, route_ids, route_weights, gate, up, down, gain, bias):
+    experts, tps = lax.axis_size("sp"), lax.axis_size("tp")
+    toks, width = normed.shape
+    need = 5 * toks // (2 * experts)
+    capacity = -(-need // 16) * 16
+    chunk = experts // 2
+    hidden_width = gate.shape[2]
+    vmem = pl.BlockSpec(memory_space=pltpu.VMEM)
+    hbm = pl.BlockSpec(memory_space=pl.ANY)
+    bf16 = jnp.bfloat16
+    dma = pltpu.SemaphoreType.DMA
+    return pl.pallas_call(
+        functools.partial(moe_kernel, experts, tps, chunk),
+        out_shape=jax.ShapeDtypeStruct((toks, width), bf16),
+        in_specs=[vmem] * 5 + [hbm] * 3,
+        out_specs=vmem,
+        scratch_shapes=[
+            pltpu.VMEM((experts, capacity, width), bf16),
+            pltpu.VMEM((experts, tps, capacity, width), bf16),
+            pltpu.VMEM((width, hidden_width), bf16),
+            pltpu.VMEM((width, hidden_width), bf16),
+            pltpu.VMEM((hidden_width, width), bf16),
+            pltpu.VMEM((chunk * tps * capacity, hidden_width), bf16),
+            pltpu.VMEM((experts, tps, capacity, width), bf16),
+            pltpu.VMEM((experts, tps, capacity, width), bf16),
+            pltpu.VMEM((experts, capacity, width), bf16),
+            pltpu.VMEM((experts, capacity, width), bf16),
+            dma((3,)),
+            dma((experts,)),
+            dma((experts,)),
+            dma((experts, tps)),
+            dma((experts, tps)),
+            dma((experts, tps)),
+            dma((experts, tps)),
+            dma((experts,)),
+            dma((experts,)),
+        ],
+        compiler_params=pltpu.CompilerParams(
+            collective_id=0, has_side_effects=True, vmem_limit_bytes=60 * 1024 * 1024
+        ),
+    )(normed, route_ids, route_weights, gain[None, :], bias[None, :], gate, up, down)
 
 
 def per_device(
@@ -87,55 +373,17 @@
         "kgqj,jkd->qkgd", weights, value_heads, preferred_element_type=jnp.float32
     )
     attended = attended.astype(jnp.bfloat16).reshape(tok_dev, local_heads * HEAD_DIM)
-    tp_size = lax.axis_size("tp")
-    tok_sub = resid.shape[0]
-    row_block = attended
     projected = lax.psum_scatter(
-        jnp.dot(row_block, out_proj, preferred_element_type=jnp.float32).astype(jnp.bfloat16),
+        jnp.dot(attended, out_proj, preferred_element_type=jnp.float32).astype(jnp.bfloat16),
         "tp",
         scatter_dimension=0,
         tiled=True,
     )
     pre_norm = residual_scale * resid.astype(jnp.float32) + projected.astype(jnp.float32)
     normed = layer_norm(pre_norm, norm1_gain, norm1_bias).astype(jnp.bfloat16)
-    experts = lax.axis_size("sp")
-    capacity = 5 * tok_sub // (2 * experts)
-    width = normed.shape[1]
-    flat_ids = route_ids.reshape(-1)
-    one_hot = (flat_ids[:, None] == jnp.arange(experts, dtype=jnp.int32)[None, :]).astype(jnp.int32)
-    ranks = jnp.cumsum(one_hot, axis=0) - 1
-    slot_rank = jnp.sum(ranks * one_hot, axis=1)
-    slots = flat_ids * capacity + slot_rank
-    assignment = slots[None, :] == jnp.arange(experts * capacity, dtype=jnp.int32)[:, None]
-    assignment = assignment.reshape(experts * capacity, tok_sub, -1).any(-1).astype(jnp.bfloat16)
-    dispatch = jnp.dot(assignment, normed, preferred_element_type=jnp.float32).astype(jnp.bfloat16)
-    dispatch = dispatch.reshape(experts, capacity, width)
-    copies = jnp.broadcast_to(dispatch[:, None], (experts, tp_size, capacity, width))
-    copies = copies.reshape(experts * tp_size, capacity, width)
-    arrived = lax.all_to_all(copies, ("sp", "tp"), split_axis=0, concat_axis=0, tiled=True)
-    arrived = arrived.reshape(experts, tp_size, capacity, width).transpose(1, 0, 2, 3)
-    flat_rows = arrived.reshape(-1, width)
-    gate_weight = expert_gate[0]
-    up_weight = expert_up[0]
-    down_weight = expert_down[0]
-    row_block = flat_rows
-    gate_act = jnp.dot(row_block, gate_weight, preferred_element_type=jnp.float32)
-    up_act = jnp.dot(row_block, up_weight, preferred_element_type=jnp.float32)
-    hidden = (jax.nn.silu(gate_act) * up_act).astype(jnp.bfloat16)
-    expert_out = lax.psum_scatter(
-        jnp.dot(hidden, down_weight, preferred_element_type=jnp.float32).astype(jnp.bfloat16),
-        "tp",
-        scatter_dimension=0,
-        tiled=True,
-    )
-    returned = lax.all_to_all(
-        expert_out.reshape(experts, capacity, width), "sp", split_axis=0, concat_axis=0, tiled=True
-    )
-    gathered = jnp.take(returned.reshape(experts * capacity, width), slots, axis=0)
-    gathered = gathered.reshape(tok_sub, -1, width).astype(jnp.float32)
-    moe_sum = jnp.sum(route_weights[:, :, None] * gathered, axis=1)
-    pre_final = residual_scale * normed.astype(jnp.float32) + moe_sum
-    return layer_norm(pre_final, norm2_gain, norm2_bias).astype(jnp.bfloat16)
+    return run_moe(
+        normed, route_ids, route_weights, expert_gate, expert_up, expert_down, norm2_gain, norm2_bias
+    )
 
 
 def solution(mesh):

time: 230 us -> 159 us (0.69)
  the two profiles are of different devices: /device:TPU:0 before, /device:TPU:17 now
where the time goes in v1:
time: 159 us; the launch traced here: 158 us
  Pallas kernels  87.4 us (55%)
  waiting for transfers between devices  17 us (11%)
  starting transfers between devices  16.8 us (11%)
  between operations  13.7 us (9%)
  local copies, waits for them, and re-layouts  9.44 us (6%)
  other arithmetic  8.25 us (5%)
  matrix products  5.41 us (3%)
    pallas_call x1, Pallas kernels, run_moe(): pl.pallas_call(functools.partial(moe_kernel, experts, tps, chunk), out_sh...  87.4 us
    reduce_scatter x1, waiting for transfers between devices, per_device(): lax.psum_scatter(jnp.dot(attended, out_proj, preferred_element_type=jnp.f...  17 us
    ppermute x3, starting transfers between devices, with_halo(): lax.ppermute(tail, axis, [(i, (i + 1) % count) for i in range(ends)])  11 us
    unnamed x20, local copies, waits for them, and re-layouts  5.88 us
    ppermute x3, starting transfers between devices, with_halo(): lax.ppermute(head, axis, [((i + 1) % count, i) for i in range(ends)])  5.75 us
  transfers between devices with their start and end apart: 7, of which 1 were waited for; matrix products, arithmetic and copies ran while one was open for 6% of the time, Pallas kernels for 0%

profile of v1, /device:TPU:17, one launch (start us, length us, event | category | flops | bytes accessed | tf_op | source)
XLA Modules:
  0.0 158.0 jit_solution(10479218472372947204)
XLA Ops:
  6.5 0.0 copy-start
  6.5 0.0 reduce-scatter.2.cloned.1.call-start
  6.5 0.9 fusion.12
  7.5 3.8 %collective-permute-start.2 = (s32[128]{0:T(128)S(1)}, s32[128]{0:T(128)S(1)}, u32[]{:S(2)}, u32[]{:S(2)}) collective-permute-start(s32[128]{0:T(128)S(1)} %get-tuple-element.9), channel_id=1, source_target_pairs={{0,2},{2,4},{4,6},{6,8},{8,10},{10,12},{12,14},{1,3},{3,5},{5,7},{... | collective-permute-start | bytes 1544 | tf_op jit(solution)/shard_map/ppermute | solution.py:28
  11.2 1.9 %collective-permute-start.3 = (s32[128]{0:T(128)S(1)}, s32[128]{0:T(128)S(1)}, u32[]{:S(2)}, u32[]{:S(2)}) collective-permute-start(s32[128]{0:T(128)S(1)} %get-tuple-element.10), channel_id=1, source_target_pairs={{2,0},{4,2},{6,4},{8,6},{10,8},{12,10},{14,12},{3,1},{5,3},{7,5},{... | collective-permute-start | bytes 1544 | tf_op jit(solution)/shard_map/ppermute | solution.py:30
  13.1 0.8 fusion.10
  14.0 3.6 %collective-permute-start.4 = (bf16[128,128]{1,0:T(8,128)(2,1)S(1)}, bf16[128,128]{1,0:T(8,128)(2,1)S(1)}, u32[]{:S(2)}, u32[]{:S(2)}) collective-permute-start(bf16[128,128]{1,0:T(8,128)(2,1)S(1)} %get-tuple-element.5), channel_id=1, source_target_pairs={{0,2},{2,4},{4,6},{6,8},{8,10},{10,12},{12,14},{1,3},{3,5},{5,7},{... | collective-permute-start | bytes 98312 | tf_op jit(solution)/shard_map/ppermute | solution.py:28
  17.6 1.9 %collective-permute-start.5 = (bf16[128,128]{1,0:T(8,128)(2,1)S(1)}, bf16[128,128]{1,0:T(8,128)(2,1)S(1)}, u32[]{:S(2)}, u32[]{:S(2)}) collective-permute-start(bf16[128,128]{1,0:T(8,128)(2,1)S(1)} %get-tuple-element.6), channel_id=1, source_target_pairs={{2,0},{4,2},{6,4},{8,6},{10,8},{12,10},{14,12},{3,1},{5,3},{7,5},{... | collective-permute-start | bytes 98312 | tf_op jit(solution)/shard_map/ppermute | solution.py:30
  19.6 0.8 fusion.11
  20.4 3.6 %collective-permute-start = (bf16[128,128]{1,0:T(8,128)(2,1)S(1)}, bf16[128,128]{1,0:T(8,128)(2,1)S(1)}, u32[]{:S(2)}, u32[]{:S(2)}) collective-permute-start(bf16[128,128]{1,0:T(8,128)(2,1)S(1)} %get-tuple-element.7), channel_id=1, source_target_pairs={{0,2},{2,4},{4,6},{6,8},{8,10},{10,12},{12,14},{1,3},{3,5},{5,7},{... | collective-permute-start | bytes 98312 | tf_op jit(solution)/shard_map/ppermute | solution.py:28
  24.1 1.1 copy.24
  25.1 0.7 max.18
  25.9 0.0 collective-permute-done.2
  25.9 1.9 %collective-permute-start.1 = (bf16[128,128]{1,0:T(8,128)(2,1)S(1)}, bf16[128,128]{1,0:T(8,128)(2,1)S(1)}, u32[]{:S(2)}, u32[]{:S(2)}) collective-permute-start(bf16[128,128]{1,0:T(8,128)(2,1)S(1)} %get-tuple-element.8), channel_id=1, source_target_pairs={{2,0},{4,2},{6,4},{8,6},{10,8},{12,10},{14,12},{3,1},{5,3},{7,5},{... | collective-permute-start | bytes 98312 | tf_op jit(solution)/shard_map/ppermute | solution.py:30
  27.8 0.0 collective-permute-done.3
  27.8 0.8 pad_add_fusion
  28.6 0.9 fusion.6
  29.5 0.0 collective-permute-done.4
  29.5 0.0 collective-permute-done.5
  29.5 0.8 pad_maximum_fusion.1
  30.3 0.1 copy.23
  30.4 0.0 copy-start.3
  30.4 0.9 fusion
  31.3 0.0 copy-start.1
  31.3 0.1 broadcast_maximum_fusion
  31.4 1.6 copy-done.1
  33.0 1.1 fusion.1
  34.1 0.1 exponential_add_fusion
  34.2 0.0 collective-permute-done
  34.2 0.0 collective-permute-done.1
  34.2 0.0 copy-done.3
  34.2 0.1 copy.22
  34.3 3.0 %fusion.3 = bf16[2,64,4,192]{3,1,2,0:T(8,128)(2,1)S(1)} fusion(bf16[448,2,64,1]{0,2,3,1:T(8,128)(2,1)S(1)} %bitcast.37, f32[2,448,192,4]{1,2,3,0:T(8,128)} %copy-done.1, f32[2,4,192]{2,1,0:T(4,128)S(1)} %exponential_add_fusion, f32[2,4,192]{2,1,0:T(4,128)S(1)} %broadcast_maximum_fusion, pred[192,448]{1,0:T(8,128)(4,1)S(1)} %fusion.6), kind=kOutput, calls=%fused_computation.7 | convolution fusion | flops 92307456 | bytes 3162112 | tf_op jit(solution)/shard_map/kgqj,jkd->qkgd/dot_general | solution.py:372
  37.4 0.0 copy-start.6
  37.4 0.0 copy-start.7
  37.4 0.0 copy-start.2
  37.4 0.0 copy-start.4
  37.4 0.0 copy-start.5
  37.4 0.0 copy-done
  37.4 1.5 convolution_convert_fusion
  38.9 0.0 reduce-scatter.2.cloned.1.call-update
  39.0 0.0 copy-done.6
  39.0 0.7 copy.25.ids_ref
  39.7 0.0 copy-done.7
  39.7 0.7 copy.26.rw_ref
  40.4 17.0 %reduce-scatter.2.cloned.1.call-done = bf16[96,2048]{1,0:T(8,128)(2,1)} async-done(((bf16[192,2048]{1,0:T(8,128)(2,1)}), bf16[96,2048]{1,0:T(8,128)(2,1)}) %reduce-scatter.2.cloned.1.call-update) | async-done | bytes 393232 | tf_op jit(solution)/shard_map/reduce_scatter | solution.py:376
  57.4 0.0 copy-done.2
  57.4 1.2 fusion.4
  58.7 1.3 multiply_reduce_fusion
  60.0 0.0 copy-done.4
  60.0 0.0 copy-done.5
  60.0 2.0 %add_convert_fusion.normed_ref = bf16[96,2048]{1,0:T(8,128)(2,1)} fusion(bf16[96,2048]{1,0:T(8,128)(2,1)} %reduce-scatter.2.cloned.1.call-done, bf16[96,2048]{1,0:T(8,128)(2,1)S(1)} %copy-done.2, f32[2048]{0:T(1024)S(1)} %copy-done.4, f32[2048]{0:T(1024)S(1)} %copy-done.5, f32[96]{0:T(128)S(1)} %add_rsqrt_fusion, f32[96]{0:T(128)S(1)} %broadcast_multiply_fusion), kind=kLoop, calls=%fused_computation.8 | loop fusion | flops 1769472 | bytes 1196800 | tf_op jit(solution)/shard_map/convert_element_type | solution.py:383
  62.0 87.4 %shard_map.154 = bf16[96,2048]{1,0:T(8,128)(2,1)} custom-call(bf16[96,2048]{1,0:T(8,128)(2,1)} %add_convert_fusion.normed_ref, s32[96,2]{1,0:T(8,128)} %copy.25.ids_ref, f32[96,2]{1,0:T(8,128)} %copy.26.rw_ref, f32[1,2048]{1,0:T(1,128)} %bitcast.38, f32[1,2048]{1,0:T(1,128)} %bitcast.39, bf16[1,2048,1536]{2,1,0:T(8,128)(2,1)} %gate_hbm.1, ...), custom_call_target="tpu_custom_call" | custom-call | tf_op jit(solution)/shard_map/pallas_call | solution.py:293
  149.4 1.8 %copy.30 = bf16[96,2048]{1,0:T(8,128)(2,1)} copy(bf16[96,2048]{1,0:T(8,128)(2,1)} %shard_map.154) | data formatting | bytes 786432
  (6 shorter events, 0.0 us)
Async XLA Ops:
  6.5 30.9 %copy-start = (bf16[512,2048]{1,0:T(8,128)(2,1)S(1)}, bf16[512,2048]{1,0:T(8,128)(2,1)}, u32[]{:S(2)}) copy-start(bf16[512,2048]{1,0:T(8,128)(2,1)} %param.22) | copy-start | bytes 6291460
  6.5 50.9 %reduce-scatter.2.cloned.1.call-start = ((), (), s32[]{:S(2)}) async-start(), calls=%async_computation.1 | async-start | bytes 1179648 | tf_op jit(solution)/shard_map/reduce_scatter | solution.py:376
  7.5 18.4 %collective-permute-start.2 = (s32[128]{0:T(128)S(1)}, s32[128]{0:T(128)S(1)}, u32[]{:S(2)}, u32[]{:S(2)}) collective-permute-start(s32[128]{0:T(128)S(1)} %get-tuple-element.9), channel_id=1, source_target_pairs={{0,2},{2,4},{4,6},{6,8},{8,10},{10,12},{12,14},{1,3},{3,5},{5,7},{... | collective-permute-start | bytes 1544 | tf_op jit(solution)/shard_map/ppermute | solution.py:28
  11.2 16.6 %collective-permute-start.3 = (s32[128]{0:T(128)S(1)}, s32[128]{0:T(128)S(1)}, u32[]{:S(2)}, u32[]{:S(2)}) collective-permute-start(s32[128]{0:T(128)S(1)} %get-tuple-element.10), channel_id=1, source_target_pairs={{2,0},{4,2},{6,4},{8,6},{10,8},{12,10},{14,12},{3,1},{5,3},{7,5},{... | collective-permute-start | bytes 1544 | tf_op jit(solution)/shard_map/ppermute | solution.py:30
  14.0 15.5 %collective-permute-start.4 = (bf16[128,128]{1,0:T(8,128)(2,1)S(1)}, bf16[128,128]{1,0:T(8,128)(2,1)S(1)}, u32[]{:S(2)}, u32[]{:S(2)}) collective-permute-start(bf16[128,128]{1,0:T(8,128)(2,1)S(1)} %get-tuple-element.5), channel_id=1, source_target_pairs={{0,2},{2,4},{4,6},{6,8},{8,10},{10,12},{12,14},{1,3},{3,5},{5,7},{... | collective-permute-start | bytes 98312 | tf_op jit(solution)/shard_map/ppermute | solution.py:28
  17.6 11.9 %collective-permute-start.5 = (bf16[128,128]{1,0:T(8,128)(2,1)S(1)}, bf16[128,128]{1,0:T(8,128)(2,1)S(1)}, u32[]{:S(2)}, u32[]{:S(2)}) collective-permute-start(bf16[128,128]{1,0:T(8,128)(2,1)S(1)} %get-tuple-element.6), channel_id=1, source_target_pairs={{2,0},{4,2},{6,4},{8,6},{10,8},{12,10},{14,12},{3,1},{5,3},{7,5},{... | collective-permute-start | bytes 98312 | tf_op jit(solution)/shard_map/ppermute | solution.py:30
  20.4 13.8 %collective-permute-start = (bf16[128,128]{1,0:T(8,128)(2,1)S(1)}, bf16[128,128]{1,0:T(8,128)(2,1)S(1)}, u32[]{:S(2)}, u32[]{:S(2)}) collective-permute-start(bf16[128,128]{1,0:T(8,128)(2,1)S(1)} %get-tuple-element.7), channel_id=1, source_target_pairs={{0,2},{2,4},{4,6},{6,8},{8,10},{10,12},{12,14},{1,3},{3,5},{5,7},{... | collective-permute-start | bytes 98312 | tf_op jit(solution)/shard_map/ppermute | solution.py:28
  25.9 8.3 %collective-permute-start.1 = (bf16[128,128]{1,0:T(8,128)(2,1)S(1)}, bf16[128,128]{1,0:T(8,128)(2,1)S(1)}, u32[]{:S(2)}, u32[]{:S(2)}) collective-permute-start(bf16[128,128]{1,0:T(8,128)(2,1)S(1)} %get-tuple-element.8), channel_id=1, source_target_pairs={{2,0},{4,2},{6,4},{8,6},{10,8},{12,10},{14,12},{3,1},{5,3},{7,5},{... | collective-permute-start | bytes 98312 | tf_op jit(solution)/shard_map/ppermute | solution.py:30
  30.4 3.8 %copy-start.3 = (bf16[192,128]{1,0:T(8,128)(2,1)S(1)}, bf16[192,128]{1,0:T(8,128)(2,1)}, u32[]{:S(2)}) copy-start(bf16[192,128]{1,0:T(8,128)(2,1)} %param.19) | copy-start | bytes 147460
  31.3 1.7 %copy-start.1 = (f32[2,448,192,4]{1,2,3,0:T(8,128)}, f32[2,448,192,4]{1,2,3,0:T(8,128)S(1)}, u32[]{:S(2)}) copy-start(f32[2,448,192,4]{1,2,3,0:T(8,128)S(1)} %get-tuple-element.12) | copy-start | bytes 8257540
  37.4 1.6 %copy-start.6 = (s32[96,2]{0,1:T(2,128)S(1)}, s32[96,2]{0,1:T(2,128)}, u32[]{:S(2)}) copy-start(s32[96,2]{0,1:T(2,128)} %param.25) | copy-start | bytes 2308
  37.4 2.3 %copy-start.7 = (f32[96,2]{0,1:T(2,128)S(1)}, f32[96,2]{0,1:T(2,128)}, u32[]{:S(2)}) copy-start(f32[96,2]{0,1:T(2,128)} %param.26) | copy-start | bytes 2308
  37.4 20.0 %copy-start.2 = (bf16[96,2048]{1,0:T(8,128)(2,1)S(1)}, bf16[96,2048]{1,0:T(8,128)(2,1)}, u32[]{:S(2)}) copy-start(bf16[96,2048]{1,0:T(8,128)(2,1)} %param.16) | copy-start | bytes 1179652
  37.4 22.6 %copy-start.4 = (f32[2048]{0:T(1024)S(1)}, f32[2048]{0:T(1024)}, u32[]{:S(2)}) copy-start(f32[2048]{0:T(1024)} %param.24) | copy-start | bytes 24580
  37.4 22.6 %copy-start.5 = (f32[2048]{0:T(1024)S(1)}, f32[2048]{0:T(1024)}, u32[]{:S(2)}) copy-start(f32[2048]{0:T(1024)} %param.23) | copy-start | bytes 24580
Sparse Core Ops, SparseCore 0:
  39.1 18.2 reduce-scatter.1

commit v2 on v1

--- a/solution.py
+++ b/solution.py
@@ -10,28 +10,12 @@
 HEAD_DIM = 64
 WINDOW = 128
 MESH = pl.DeviceIdType.MESH
+CHUNKS = 2
 
 
 norm_epsilon = 1e-05
 residual_scale = 1.4142135623730951
 masked_score = -1e30
-
-
-def with_halo(cells, sides, width):
-    for axis, dim in sides:
-        count = lax.axis_size(axis)
-        ends = count - 1
-        head = lax.slice_in_dim(cells, 0, width, axis=dim)
-        tail = lax.slice_in_dim(cells, cells.shape[dim] - width, cells.shape[dim], axis=dim)
-        cells = jnp.concatenate(
-            [
-                lax.ppermute(tail, axis, [(i, (i + 1) % count) for i in range(ends)]),
-                cells,
-                lax.ppermute(head, axis, [((i + 1) % count, i) for i in range(ends)]),
-            ],
-            axis=dim,
-        )
-    return cells
 
 
 def layer_norm(values, gain_vec, bias_vec):
@@ -58,19 +42,169 @@
     return target * 2 + (core + flip) % 2
 
 
-def moe_kernel(
+def head_copy(d, t, tps, head_part, head_peer, head_send, head_recv):
+    return pltpu.make_async_remote_copy(
+        src_ref=head_part.at[d],
+        dst_ref=head_peer.at[d],
+        send_sem=head_send.at[d],
+        recv_sem=head_recv.at[d],
+        device_id={"tp": (t + d) % tps},
+        device_id_type=MESH,
+    )
+
+
+def attend(
+    count,
+    tps,
+    queries_ref,
+    keys_ref,
+    values_ref,
+    docs_ref,
+    sink_ref,
+    proj_w,
+    key_pad,
+    value_pad,
+    doc_pad,
+    attended,
+    head_part,
+    head_peer,
+    halo_send,
+    halo_recv,
+    head_send,
+    head_recv,
+    barrier,
+    first_copies,
+):
+    me, t = lax.axis_index("sp"), lax.axis_index("tp")
+    tok_dev, tok_sub = queries_ref.shape[0], attended.shape[0]
+    local_kv = keys_ref.shape[1] // HEAD_DIM
+    heads = queries_ref.shape[1] // HEAD_DIM
+    groups = heads // local_kv
+    reach = -(-(tok_sub + 2 * WINDOW) // 128) * 128
+    end = WINDOW + tok_dev
+    rest = key_pad.shape[0] - end - WINDOW
+    for pad, own in ((key_pad, keys_ref), (value_pad, values_ref), (doc_pad, docs_ref)):
+        pad[WINDOW:end] = own[...]
+        if rest:
+            pad[end + WINDOW :] = jnp.zeros((rest, pad.shape[1]), pad.dtype)
+    pl.semaphore_wait(barrier, count - 1 + tps - 1)
+    copies = []
+    for i, (pad, own) in enumerate(
+        ((key_pad, keys_ref), (value_pad, values_ref), (doc_pad, docs_ref))
+    ):
+        for side in range(2):
+            start, place = (tok_dev - WINDOW, 0) if side == 0 else (0, end)
+            copies.append(
+                pltpu.make_async_remote_copy(
+                    src_ref=own.at[pl.ds(start, WINDOW)],
+                    dst_ref=pad.at[pl.ds(place, WINDOW)],
+                    send_sem=halo_send.at[2 * i + side],
+                    recv_sem=halo_recv.at[2 * i + side],
+                    device_id={"sp": (me + 1) % count if side == 0 else (me + count - 1) % count},
+                    device_id_type=MESH,
+                )
+            )
+    for copy in copies:
+        copy.start()
+    for copy in copies:
+        copy.wait_recv()
+
+    for d in list(range(1, tps)) + [0]:
+        base = pl.multiple_of((t + d) % tps * tok_sub, 16)
+        key_block = key_pad[pl.ds(base, reach), :].astype(jnp.float32)
+        value_block = value_pad[pl.ds(base, reach), :].astype(jnp.float32)
+        key_docs = jnp.transpose(doc_pad[pl.ds(base, reach), :])[0:1, :]
+        query_docs = docs_ref[pl.ds(base, tok_sub), 0:1]
+        row = lax.broadcasted_iota(jnp.int32, (tok_sub, reach), 0)
+        col = lax.broadcasted_iota(jnp.int32, (tok_sub, reach), 1)
+        position = me * tok_dev + base - WINDOW + col
+        allowed = (position >= 0) & (position < count * tok_dev)
+        allowed = allowed & (col >= row) & (col <= row + 2 * WINDOW)
+        allowed = allowed & (query_docs == key_docs)
+        blank = jnp.zeros((reach, HEAD_DIM), jnp.float32)
+        for g in range(local_kv):
+            span = slice(g * HEAD_DIM, (g + 1) * HEAD_DIM)
+            sides = []
+            for block in (key_block, value_block):
+                piece = block[:, span]
+                sides.append(
+                    [
+                        jnp.concatenate([piece, blank], 1).astype(jnp.bfloat16),
+                        jnp.concatenate([blank, piece], 1).astype(jnp.bfloat16),
+                    ]
+                )
+            for pair in range(groups // 2):
+                lane = (g * groups + 2 * pair) * HEAD_DIM
+                query = queries_ref[pl.ds(base, tok_sub), lane : lane + 2 * HEAD_DIM]
+                result = jnp.zeros((tok_sub, 2 * HEAD_DIM), jnp.float32)
+                for parity in range(2):
+                    head = g * groups + 2 * pair + parity
+                    sink = sink_ref[:, head : head + 1]
+                    scores = lax.dot_general(
+                        query,
+                        sides[0][parity],
+                        (((1,), (1,)), ((), ())),
+                        preferred_element_type=jnp.float32,
+                    )
+                    scores = jnp.where(allowed, scores * HEAD_DIM ** (-0.5), masked_score)
+                    top = jnp.maximum(jnp.max(scores, -1, keepdims=True), sink)
+                    raised = jnp.where(allowed, jnp.exp(scores - top), 0.0)
+                    total = jnp.exp(sink - top) + jnp.sum(raised, -1, keepdims=True)
+                    weights = (raised / total).astype(jnp.bfloat16)
+                    result = result + jnp.dot(
+                        weights, sides[1][parity], preferred_element_type=jnp.float32
+                    )
+                attended[:, lane : lane + 2 * HEAD_DIM] = result.astype(jnp.bfloat16)
+        if d == 1 or tps == 1:
+            for copy in first_copies:
+                copy.wait()
+        tile = 512
+        width = proj_w.shape[1]
+
+        def project(i, carry):
+            cols = pl.ds(pl.multiple_of(i * tile, tile), tile)
+            head_part[d, :, cols] = jnp.dot(
+                attended[...], proj_w[:, cols], preferred_element_type=jnp.float32
+            ).astype(jnp.bfloat16)
+            return carry
+
+        lax.fori_loop(0, width // tile, project, 0)
+        if d:
+            head_copy(d, t, tps, head_part, head_peer, head_send, head_recv).start()
+    for copy in copies:
+        copy.wait_send()
+
+
+def layer_kernel(
     experts,
     tps,
     chunk,
-    normed_ref,
+    queries_ref,
+    keys_ref,
+    values_ref,
+    docs_ref,
+    sink_ref,
+    gain1_ref,
+    bias1_ref,
     ids_ref,
     rw_ref,
     gain_ref,
     bias_ref,
+    resid_hbm,
+    proj_hbm,
     gate_hbm,
     up_hbm,
     down_hbm,
     out_ref,
+    resid_ref,
+    proj_w,
+    key_pad,
+    value_pad,
+    doc_pad,
+    attended,
+    head_part,
+    head_peer,
+    normed_ref,
     outgoing,
     rows,
     gate_w,
@@ -90,10 +224,20 @@
     part_recv,
     ret_send,
     ret_recv,
+    halo_send,
+    halo_recv,
+    head_send,
+    head_recv,
 ):
     me, t = lax.axis_index("sp"), lax.axis_index("tp")
     _, capacity, width = outgoing.shape
     toks = normed_ref.shape[0]
+    first_copies = [
+        pltpu.make_async_copy(resid_hbm, resid_ref, w_sem.at[3]),
+        pltpu.make_async_copy(proj_hbm, proj_w, w_sem.at[4]),
+    ]
+    for copy in first_copies:
+        copy.start()
     weight_copies = [
         pltpu.make_async_copy(gate_hbm.at[0], gate_w, w_sem.at[0]),
         pltpu.make_async_copy(up_hbm.at[0], up_w, w_sem.at[1]),
@@ -110,6 +254,28 @@
     for d in range(1, tps):
         pl.semaphore_signal(barrier, inc=1, device_id={"tp": (t + d) % tps}, device_id_type=MESH)
 
+    attend(
+        experts,
+        tps,
+        queries_ref,
+        keys_ref,
+        values_ref,
+        docs_ref,
+        sink_ref,
+        proj_w,
+        key_pad,
+        value_pad,
+        doc_pad,
+        attended,
+        head_part,
+        head_peer,
+        halo_send,
+        halo_recv,
+        head_send,
+        head_recv,
+        barrier,
+        first_copies,
+    )
     lanes = experts * capacity
     ids = ids_ref[...]
     wide = max(experts, 128)
@@ -131,6 +297,13 @@
         match = (own * capacity + rank == slot_iota).astype(jnp.float32)
         assign = assign + match
         combine = combine + match * rw_ref[:, k : k + 1]
+    projected = head_part[0].astype(jnp.float32)
+    for d in range(1, tps):
+        head_copy(d, t, tps, head_part, head_peer, head_send, head_recv).wait_recv()
+        projected = projected + head_peer[d].astype(jnp.float32)
+    projected = projected.astype(jnp.bfloat16).astype(jnp.float32)
+    pre_norm = residual_scale * resid_ref[...].astype(jnp.float32) + projected
+    normed_ref[...] = layer_norm(pre_norm, gain1_ref[...], bias1_ref[...]).astype(jnp.bfloat16)
     spread = lax.dot_general(
         assign.astype(jnp.bfloat16),
         normed_ref[...],
@@ -139,8 +312,6 @@
     )
     outgoing[...] = spread.astype(jnp.bfloat16).reshape(experts, capacity, width)
     rows[0, t] = outgoing[me]
-
-    pl.semaphore_wait(barrier, experts - 1 + tps - 1)
 
     def dispatch(step):
         dst = step_partner(step, me, experts, False)
@@ -270,6 +441,8 @@
     pre_final = residual_scale * normed_ref[...].astype(jnp.float32) + moe_sum
     out_ref[...] = layer_norm(pre_final, gain_ref[...], bias_ref[...]).astype(jnp.bfloat16)
 
+    for d in range(1, tps):
+        head_copy(d, t, tps, head_part, head_peer, head_send, head_recv).wait_send()
     for step in range(experts):
         if step > 0:
             dispatch(step).wait_send()
@@ -277,49 +450,6 @@
         for d in range(1, tps):
             forward(step, d).wait_send()
             share(step, d).wait_send()
-
-
-def run_moe(normed, route_ids, route_weights, gate, up, down, gain, bias):
-    experts, tps = lax.axis_size("sp"), lax.axis_size("tp")
-    toks, width = normed.shape
-    need = 5 * toks // (2 * experts)
-    capacity = -(-need // 16) * 16
-    chunk = experts // 2
-    hidden_width = gate.shape[2]
-    vmem = pl.BlockSpec(memory_space=pltpu.VMEM)
-    hbm = pl.BlockSpec(memory_space=pl.ANY)
-    bf16 = jnp.bfloat16
-    dma = pltpu.SemaphoreType.DMA
-    return pl.pallas_call(
-        functools.partial(moe_kernel, experts, tps, chunk),
-        out_shape=jax.ShapeDtypeStruct((toks, width), bf16),
-        in_specs=[vmem] * 5 + [hbm] * 3,
-        out_specs=vmem,
-        scratch_shapes=[
-            pltpu.VMEM((experts, capacity, width), bf16),
-            pltpu.VMEM((experts, tps, capacity, width), bf16),
-            pltpu.VMEM((width, hidden_width), bf16),
-            pltpu.VMEM((width, hidden_width), bf16),
-            pltpu.VMEM((hidden_width, width), bf16),
-            pltpu.VMEM((chunk * tps * capacity, hidden_width), bf16),
-            pltpu.VMEM((experts, tps, capacity, width), bf16),
-            pltpu.VMEM((experts, tps, capacity, width), bf16),
-            pltpu.VMEM((experts, capacity, width), bf16),
-            pltpu.VMEM((experts, capacity, width), bf16),
-            dma((3,)),
-            dma((experts,)),
-            dma((experts,)),
-            dma((experts, tps)),
-            dma((experts, tps)),
-            dma((experts, tps)),
-            dma((experts, tps)),
-            dma((experts,)),
-            dma((experts,)),
-        ],
-        compiler_params=pltpu.CompilerParams(
-            collective_id=0, has_side_effects=True, vmem_limit_bytes=60 * 1024 * 1024
-        ),
-    )(normed, route_ids, route_weights, gain[None, :], bias[None, :], gate, up, down)
 
 
 def per_device(
@@ -340,49 +470,79 @@
     norm2_gain,
     norm2_bias,
 ):
-    tok_dev = queries.shape[0]
-    local_kv = keys.shape[1] // HEAD_DIM
-    local_heads = queries.shape[1] // HEAD_DIM
-    groups = local_heads // local_kv
-    reach = tok_dev + 2 * WINDOW
-    padded_keys, padded_values, padded_docs = (
-        with_halo(keys, (("sp", 0),), WINDOW),
-        with_halo(values, (("sp", 0),), WINDOW),
-        with_halo(doc_ids, (("sp", 0),), WINDOW),
-    )
-    offset = lax.axis_index("sp") * tok_dev
-    seq_total = lax.axis_size("sp") * tok_dev
-    query_pos = offset + jnp.arange(tok_dev, dtype=jnp.int32)
-    key_pos = offset - WINDOW + jnp.arange(reach, dtype=jnp.int32)
-    allowed = (key_pos[None, :] >= 0) & (key_pos[None, :] < seq_total)
-    allowed = allowed & (jnp.abs(query_pos[:, None] - key_pos[None, :]) <= WINDOW)
-    allowed = allowed & (doc_ids[:, None] == padded_docs[None, :])
-    query_heads = queries.reshape(tok_dev, local_kv, groups, HEAD_DIM)
-    key_heads = padded_keys.reshape(reach, local_kv, HEAD_DIM)
-    value_heads = padded_values.reshape(reach, local_kv, HEAD_DIM)
-    sink_local = sink_logits.reshape(local_kv, groups, 1, 1)
-    scores = jnp.einsum(
-        "qkgd,jkd->kgqj", query_heads, key_heads, preferred_element_type=jnp.float32
-    )
-    scores = jnp.where(allowed, scores * HEAD_DIM ** (-0.5), masked_score)
-    top_score = jnp.maximum(jnp.max(scores, -1, keepdims=True), sink_local)
-    raised = jnp.where(allowed, jnp.exp(scores - top_score), 0.0)
-    denominator = jnp.exp(sink_local - top_score) + jnp.sum(raised, -1, keepdims=True)
-    weights = (raised / denominator).astype(jnp.bfloat16)
-    attended = jnp.einsum(
-        "kgqj,jkd->qkgd", weights, value_heads, preferred_element_type=jnp.float32
-    )
-    attended = attended.astype(jnp.bfloat16).reshape(tok_dev, local_heads * HEAD_DIM)
-    projected = lax.psum_scatter(
-        jnp.dot(attended, out_proj, preferred_element_type=jnp.float32).astype(jnp.bfloat16),
-        "tp",
-        scatter_dimension=0,
-        tiled=True,
-    )
-    pre_norm = residual_scale * resid.astype(jnp.float32) + projected.astype(jnp.float32)
-    normed = layer_norm(pre_norm, norm1_gain, norm1_bias).astype(jnp.bfloat16)
-    return run_moe(
-        normed, route_ids, route_weights, expert_gate, expert_up, expert_down, norm2_gain, norm2_bias
+    experts, tps = lax.axis_size("sp"), lax.axis_size("tp")
+    toks, width = resid.shape
+    tok_dev, kv_width = keys.shape
+    need = 5 * toks // (2 * experts)
+    capacity = -(-need // 16) * 16
+    chunk = experts // CHUNKS
+    hidden_width = expert_gate.shape[2]
+    reach = -(-(toks + 2 * WINDOW) // 128) * 128
+    padded = (tps - 1) * toks + reach
+    docs = jnp.broadcast_to(doc_ids[:, None], (tok_dev, 128))
+    vmem = pl.BlockSpec(memory_space=pltpu.VMEM)
+    hbm = pl.BlockSpec(memory_space=pl.ANY)
+    bf16 = jnp.bfloat16
+    dma = pltpu.SemaphoreType.DMA
+    return pl.pallas_call(
+        functools.partial(layer_kernel, experts, tps, chunk),
+        out_shape=jax.ShapeDtypeStruct((toks, width), bf16),
+        in_specs=[vmem] * 11 + [hbm] * 5,
+        out_specs=vmem,
+        scratch_shapes=[
+            pltpu.VMEM((toks, width), bf16),
+            pltpu.VMEM(out_proj.shape, bf16),
+            pltpu.VMEM((padded, kv_width), bf16),
+            pltpu.VMEM((padded, kv_width), bf16),
+            pltpu.VMEM((padded, 128), jnp.int32),
+            pltpu.VMEM((toks, queries.shape[1]), bf16),
+            pltpu.VMEM((tps, toks, width), bf16),
+            pltpu.VMEM((tps, toks, width), bf16),
+            pltpu.VMEM((toks, width), bf16),
+            pltpu.VMEM((experts, capacity, width), bf16),
+            pltpu.VMEM((experts, tps, capacity, width), bf16),
+            pltpu.VMEM((width, hidden_width), bf16),
+            pltpu.VMEM((width, hidden_width), bf16),
+            pltpu.VMEM((hidden_width, width), bf16),
+            pltpu.VMEM((chunk * tps * capacity, hidden_width), bf16),
+            pltpu.VMEM((experts, tps, capacity, width), bf16),
+            pltpu.VMEM((experts, tps, capacity, width), bf16),
+            pltpu.VMEM((experts, capacity, width), bf16),
+            pltpu.VMEM((experts, capacity, width), bf16),
+            dma((5,)),
+            dma((experts,)),
+            dma((experts,)),
+            dma((experts, tps)),
+            dma((experts, tps)),
+            dma((experts, tps)),
+            dma((experts, tps)),
+            dma((experts,)),
+            dma((experts,)),
+            dma((6,)),
+            dma((6,)),
+            dma((tps,)),
+            dma((tps,)),
+        ],
+        compiler_params=pltpu.CompilerParams(
+            collective_id=0, has_side_effects=True, vmem_limit_bytes=60 * 1024 * 1024
+        ),
+    )(
+        queries,
+        keys,
+        values,
+        docs,
+        sink_logits[None, :],
+        norm1_gain[None, :],
+        norm1_bias[None, :],
+        route_ids,
+        route_weights,
+        norm2_gain[None, :],
+        norm2_bias[None, :],
+        resid,
+        out_proj,
+        expert_gate,
+        expert_up,
+        expert_down,
     )
 
 

time: 159 us -> 114 us (0.72)
  Pallas kernels: 87.4 us -> 107 us
  waiting for transfers between devices: 17 us -> 0 us
  starting transfers between devices: 16.8 us -> 0 us
  between operations: 13.7 us -> 0.01 us
  other arithmetic: 8.25 us -> 0 us
  matrix products: 5.41 us -> 0 us
  local copies, waits for them, and re-layouts: 9.44 us -> 5.95 us
    pallas_call x1, Pallas kernels: 87.4 us -> 107 us  [per_device(): pl.pallas_call(functools.partial(layer_kernel, experts, tps, chunk), out_...]
    reduce_scatter x1 -> x0, waiting for transfers between devices: 17 us -> none  [per_device(): lax.psum_scatter(jnp.dot(attended, out_proj, preferred_element_type=jnp.f...]
    ppermute x6 -> x0, starting transfers between devices: 16.8 us -> none  [the longest x3 11 us: with_halo(): lax.ppermute(tail, axis, [(i, (i + 1) % count) for i in range(ends)])]
    dot_general x3 -> x0, matrix products: 5.41 us -> none  [the longest x1 3.02 us: per_device(): jnp.einsum('kgqj,jkd->qkgd', weights, value_heads, preferred_element_type...]
    reduce_sum x3 -> x0, other arithmetic: 3.61 us -> none  [the longest x1 1.28 us: layer_norm(): variance = jnp.mean(centred * centred, -1, keepdims=True)]
    slice x3 -> x0, local copies, waits for them, and re-layouts: 2.6 us -> none  [with_halo(): lax.slice_in_dim(cells, cells.shape[dim] - width, cells.shape[dim], axis=...]
    convert_element_type x1 -> x0, other arithmetic: 1.99 us -> none  [per_device(): normed = layer_norm(pre_norm, norm1_gain, norm1_bias).astype(jnp.bfloat16)]
    unnamed x20 -> x3, local copies, waits for them, and re-layouts: 5.88 us -> 4.54 us
  transfers between devices with their start and end apart: 7 -> 0, of which waited for: 1 -> 0; matrix products, arithmetic and copies ran while one was open for 6% -> 0% of each run, Pallas kernels for 0% -> 0%
where the time goes in v2:
time: 114 us; the launch traced here: 113 us
  Pallas kernels  107 us (94%)
  local copies, waits for them, and re-layouts  5.95 us (5%)
    pallas_call x1, Pallas kernels, per_device(): pl.pallas_call(functools.partial(layer_kernel, experts, tps, chunk), out_...  107 us
    unnamed x3, local copies, waits for them, and re-layouts  4.54 us

profile of v2, /device:TPU:17, one launch (start us, length us, event | category | flops | bytes accessed | tf_op | source)
XLA Modules:
  0.0 113.3 jit_solution(373893870753227039)
XLA Ops:
  0.0 1.4 %copy.17.ids_ref = s32[96,2]{1,0:T(8,128)} copy(s32[96,2]{0,1:T(2,128)} %param.25) | data formatting | bytes 1536 | tf_op args[9]
  1.4 1.4 %copy.18.rw_ref = f32[96,2]{1,0:T(8,128)} copy(f32[96,2]{0,1:T(2,128)} %param.26) | data formatting | bytes 1536 | tf_op args[10]
  2.8 1.4 %broadcast_in_dim.21.docs_ref = s32[192,128]{1,0:T(8,128)} broadcast(s32[192]{0:T(256)} %param.20), dimensions={0} | broadcast | bytes 99072 | tf_op jit(solution)/shard_map/broadcast_in_dim | solution.py:482
  4.2 107.3 %shard_map.154 = bf16[96,2048]{1,0:T(8,128)(2,1)} custom-call(bf16[192,512]{1,0:T(8,128)(2,1)} %queries_ref.1, bf16[192,128]{1,0:T(8,128)(2,1)} %keys_ref.1, bf16[192,128]{1,0:T(8,128)(2,1)} %values_ref.1, s32[192,128]{1,0:T(8,128)} %broadcast_in_dim.21.docs_ref, f32[1,8]{1,0:T(1,128)} %bitcast.9, f32[1,2048]{1,0:T(1,128)} %bitcast.5, f32[1,2048]{1,0:T(1,128)} %bitcast.6, ...), custom_call_target="tpu_custom_call" | custom-call | tf_op jit(solution)/shard_map/pallas_call | solution.py:487
  111.5 1.8 %copy.20 = bf16[96,2048]{1,0:T(8,128)(2,1)} copy(bf16[96,2048]{1,0:T(8,128)(2,1)} %shard_map.154) | data formatting | bytes 786432

commit v3 on v2

--- a/solution.py
+++ b/solution.py
@@ -10,7 +10,7 @@
 HEAD_DIM = 64
 WINDOW = 128
 MESH = pl.DeviceIdType.MESH
-CHUNKS = 2
+CHUNKS = 4
 
 
 norm_epsilon = 1e-05
@@ -186,8 +186,7 @@
     sink_ref,
     gain1_ref,
     bias1_ref,
-    ids_ref,
-    rw_ref,
+    route_ref,
     gain_ref,
     bias_ref,
     resid_hbm,
@@ -277,7 +276,8 @@
         first_copies,
     )
     lanes = experts * capacity
-    ids = ids_ref[...]
+    top = route_ref.shape[1] // 2
+    ids = route_ref[:, :top].astype(jnp.int32)
     wide = max(experts, 128)
     expert_iota = lax.broadcasted_iota(jnp.int32, (toks, wide), 1)
     lower = (
@@ -296,7 +296,7 @@
         before = before + jnp.sum(hot, axis=0, keepdims=True)
         match = (own * capacity + rank == slot_iota).astype(jnp.float32)
         assign = assign + match
-        combine = combine + match * rw_ref[:, k : k + 1]
+        combine = combine + match * route_ref[:, top + k : top + k + 1]
     projected = head_part[0].astype(jnp.float32)
     for d in range(1, tps):
         head_copy(d, t, tps, head_part, head_peer, head_send, head_recv).wait_recv()
@@ -377,15 +377,16 @@
             summed[step] = total.astype(jnp.bfloat16)
             give_back(step).start()
 
-    tile = 256
+    tile = 512 if gate_w.shape[1] % 512 == 0 else 256
     hidden_width = gate_w.shape[1]
     m = chunk * tps * capacity
     chunks = experts // chunk
 
     for c in range(chunks):
         k0, k1 = c * chunk, (c + 1) * chunk
-        for step in range(k0, k1):
-            send_on(step)
+        if c == 0:
+            for step in range(k0, k1):
+                send_on(step)
         for step in range(k0, k1):
             for d in range(1, tps):
                 forward(step, d).wait_recv()
@@ -402,6 +403,9 @@
             return carry
 
         lax.fori_loop(0, hidden_width // tile, up_tile, 0)
+        if c + 1 < chunks:
+            for step in range(k1, k1 + chunk):
+                send_on(step)
         if c == 0:
             weight_copies[2].wait()
 
@@ -480,6 +484,7 @@
     reach = -(-(toks + 2 * WINDOW) // 128) * 128
     padded = (tps - 1) * toks + reach
     docs = jnp.broadcast_to(doc_ids[:, None], (tok_dev, 128))
+    routes = jnp.concatenate([route_ids.astype(jnp.float32), route_weights], 1)
     vmem = pl.BlockSpec(memory_space=pltpu.VMEM)
     hbm = pl.BlockSpec(memory_space=pl.ANY)
     bf16 = jnp.bfloat16
@@ -487,7 +492,7 @@
     return pl.pallas_call(
         functools.partial(layer_kernel, experts, tps, chunk),
         out_shape=jax.ShapeDtypeStruct((toks, width), bf16),
-        in_specs=[vmem] * 11 + [hbm] * 5,
+        in_specs=[vmem] * 10 + [hbm] * 5,
         out_specs=vmem,
         scratch_shapes=[
             pltpu.VMEM((toks, width), bf16),
@@ -534,8 +539,7 @@
         sink_logits[None, :],
         norm1_gain[None, :],
         norm1_bias[None, :],
-        route_ids,
-        route_weights,
+        routes,
         norm2_gain[None, :],
         norm2_bias[None, :],
         resid,

time: 114 us -> 94 us (0.82)
  Pallas kernels: 107 us -> 88.3 us
  local copies, waits for them, and re-layouts: 5.95 us -> 3.9 us
  other arithmetic: 0 us -> 1.37 us
    pallas_call x1, Pallas kernels: 107 us -> 88.3 us  [per_device(): pl.pallas_call(functools.partial(layer_kernel, experts, tps, chunk), out_...]
    unnamed x3 -> x1, local copies, waits for them, and re-layouts: 4.54 us -> 1.77 us
where the time goes in v3:
time: 94 us; the launch traced here: 93.6 us
  Pallas kernels  88.3 us (94%)
  local copies, waits for them, and re-layouts  3.9 us (4%)
  other arithmetic  1.37 us (1%)
    pallas_call x1, Pallas kernels, per_device(): pl.pallas_call(functools.partial(layer_kernel, experts, tps, chunk), out_...  88.3 us

profile of v3, /device:TPU:17, one launch (start us, length us, event | category | flops | bytes accessed | tf_op | source)
XLA Modules:
  0.0 93.6 jit_solution(14249852344592509963)
XLA Ops:
  0.0 0.7 convert_element_type.3
  0.7 0.7 pad_maximum_fusion
  1.4 0.7 copy.19.route_ref
  2.1 1.4 %broadcast_in_dim.21.docs_ref = s32[192,128]{1,0:T(8,128)} broadcast(s32[192]{0:T(256)} %param.20), dimensions={0} | broadcast | bytes 99072 | tf_op jit(solution)/shard_map/broadcast_in_dim | solution.py:486
  3.5 88.3 %shard_map.154 = bf16[96,2048]{1,0:T(8,128)(2,1)} custom-call(bf16[192,512]{1,0:T(8,128)(2,1)} %queries_ref.1, bf16[192,128]{1,0:T(8,128)(2,1)} %keys_ref.1, bf16[192,128]{1,0:T(8,128)(2,1)} %values_ref.1, s32[192,128]{1,0:T(8,128)} %broadcast_in_dim.21.docs_ref, f32[1,8]{1,0:T(1,128)} %bitcast.9, f32[1,2048]{1,0:T(1,128)} %bitcast.5, f32[1,2048]{1,0:T(1,128)} %bitcast.6, ...), custom_call_target="tpu_custom_call" | custom-call | tf_op jit(solution)/shard_map/pallas_call | solution.py:492
  91.8 1.8 %copy.21 = bf16[96,2048]{1,0:T(8,128)(2,1)} copy(bf16[96,2048]{1,0:T(8,128)(2,1)} %shard_map.154) | data formatting | bytes 786432
